TPU v7x, 32 devices: a whole 2x2x4 slice. The times are simulated.
32 devices in a mesh: ep: 8 (over z, x), tp: 4 (over y, core).
Axes of the slice: x: 2, y: 2, z: 4, core: 2. Of those that a mesh axis runs over, the one named last changes fastest.
Arguments:
- tokens: bfloat16 [128, 2048], P('ep'), may hold values from -6 to 6
- lengths: int32 [128], P('ep'), may hold values from 1024 to 16384
- old_state: float32 [128, 8, 128, 128], P('ep', 'tp'), may hold values from -2 to 2
- query_weight: bfloat16 [2048, 1024], P(None, 'tp'), may hold values from -0.125 to 0.125
- key_weight: bfloat16 [2048, 1024], P(None, 'tp'), may hold values from -0.125 to 0.125
- value_weight: bfloat16 [2048, 1024], P(None, 'tp'), may hold values from -0.125 to 0.125
- gate_weight: bfloat16 [2048, 1024], P(None, 'tp'), may hold values from -0.125 to 0.125
- head_gain: float32 [1024], P('tp'), may hold values from 0.1 to 1.9
- output_weight: bfloat16 [1024, 2048], P('tp'), may hold values from -0.1875 to 0.1875
- first_gain: float32 [2048], replicated, may hold values from 0.1 to 1.9
- expert_ids: int32 [128, 6], P('ep'), may hold values from 0 to 15, all different within a row; in each aligned block of 16 rows (0 to 15, 16 to 31, ...) at most 7 rows name the same one
- expert_weights: float32 [128, 6], P('ep'), may hold values from 0.05 to 0.8
- expert_gate: bfloat16 [16, 2048, 512], P('ep', None, 'tp'), may hold values from -0.125 to 0.125
- expert_up: bfloat16 [16, 2048, 512], P('ep', None, 'tp'), may hold values from -0.125 to 0.125
- expert_down: bfloat16 [16, 512, 2048], P('ep', 'tp'), may hold values from -0.25 to 0.25
- shared_gate: bfloat16 [2048, 512], P(None, 'tp'), may hold values from -0.125 to 0.125
- shared_up: bfloat16 [2048, 512], P(None, 'tp'), may hold values from -0.125 to 0.125
- shared_down: bfloat16 [512, 2048], P('tp'), may hold values from -0.25 to 0.25
- side_gate: bfloat16 [2048], replicated, may hold values from -0.125 to 0.125
- dense_gate: bfloat16 [2048, 8192], P(None, ('ep', 'tp')), may hold values from -0.125 to 0.125
- dense_up: bfloat16 [2048, 8192], P(None, ('ep', 'tp')), may hold values from -0.125 to 0.125
- dense_down: bfloat16 [8192, 2048], P(('ep', 'tp')), may hold values from -0.25 to 0.25
- second_gain: float32 [2048], replicated, may hold values from 0.1 to 1.9
Outputs:
- layer_out: bfloat16 [128, 2048], P('ep')
- new_state: float32 [128, 8, 128, 128], P('ep', 'tp')
Inputs may be any that keep to these rules, and one draw needn't show every extreme that they name: `expert_ids`: each row names 6 different experts. Among the 16 rows of one index of ep no expert is named by more than 7 rows, a bound that some block reaches.
All inputs are finite; a program needn't handle non-finite values.
Results may differ from a plain program's by a relative error of at most 0.017.
Values may be sent and summed in bfloat16 or wider, within the bound.
A program may use at most 64 MiB of HBM per device.

v0:
```python
import jax
import jax.numpy as jnp
from jax import lax
from jax.sharding import PartitionSpec as P

HEADS = 8


NORM_EPS = 1e-05
RESIDUAL_SCALE = 2.0**0.5


def rotate(inputs, positions):
    half_size = inputs.shape[-1] // 2
    frequency = 1.0 / 10000.0 ** (jnp.arange(half_size, dtype=jnp.float32) * 2.0 / inputs.shape[-1])
    angles = positions.astype(jnp.float32)[:, None] * frequency[None, :]
    cosine = jnp.cos(angles)[:, None, :]
    sine_part = jnp.sin(angles)[:, None, :]
    first_half = inputs[..., :half_size]
    second_half = inputs[..., half_size:]
    return jnp.concatenate(
        [
            first_half * cosine - second_half * sine_part,
            first_half * sine_part + second_half * cosine,
        ],
        axis=-1,
    )


def layer_norm(inputs, scale_gain):
    average = jnp.mean(inputs, axis=-1, keepdims=True)
    centered = inputs - average
    variance = jnp.mean(centered * centered, axis=-1, keepdims=True)
    return centered * lax.rsqrt(variance + NORM_EPS) * scale_gain


def expert_partial(arrived, expert_gate, expert_up, expert_down):
    gate_part = jnp.einsum(
        "secd,edf->secf", arrived, expert_gate, preferred_element_type=jnp.float32
    )
    up_part = jnp.einsum("secd,edf->secf", arrived, expert_up, preferred_element_type=jnp.float32)
    hidden = (jax.nn.silu(gate_part) * up_part).astype(jnp.bfloat16)
    return jnp.einsum("secf,efd->secd", hidden, expert_down, preferred_element_type=jnp.float32)


def route_experts(after_mixer, expert_ids, expert_weights, expert_gate, expert_up, expert_down):
    row_count, model_width = after_mixer.shape
    top_count = expert_ids.shape[1]
    local_experts = expert_gate.shape[0]
    ep_size = lax.axis_size("ep")
    tp_size = lax.axis_size("tp")
    total_experts = local_experts * ep_size
    capacity = max(2, row_count * top_count // total_experts + 1)
    flat_ids = expert_ids.reshape(-1)
    onehot = (flat_ids[:, None] == jnp.arange(total_experts, dtype=jnp.int32)[None, :]).astype(
        jnp.int32
    )
    slot_rank = jnp.sum(onehot * (jnp.cumsum(onehot, axis=0) - 1), axis=1)
    targets = flat_ids * capacity + slot_rank
    placing = (
        jnp.arange(total_experts * capacity, dtype=jnp.int32)[:, None] == targets[None, :]
    ).astype(jnp.bfloat16)
    repeated = jnp.repeat(after_mixer, top_count, axis=0)
    outgoing = jnp.dot(placing, repeated, preferred_element_type=jnp.float32).astype(jnp.bfloat16)
    outgoing = outgoing.reshape(ep_size, local_experts, capacity, model_width)
    column_width = model_width // tp_size
    own_cols = lax.dynamic_slice_in_dim(
        outgoing, lax.axis_index("tp") * column_width, column_width, 3
    )
    arrived = lax.all_to_all(own_cols, "ep", split_axis=0, concat_axis=0, tiled=True)
    whole_rows = lax.all_gather(arrived, "tp", axis=3, tiled=True)
    outputs = expert_partial(whole_rows, expert_gate, expert_up, expert_down)
    reduced = lax.psum_scatter(outputs.astype(jnp.bfloat16), "tp", scatter_dimension=3, tiled=True)
    came_back = lax.all_to_all(reduced, "ep", split_axis=0, concat_axis=0, tiled=True)
    returned = lax.all_gather(came_back, "tp", axis=3, tiled=True)
    returned = returned.reshape(total_experts * capacity, model_width)
    gathered_back = jnp.dot(placing.T, returned, preferred_element_type=jnp.float32)
    weighted = gathered_back.reshape(row_count, top_count, model_width) * expert_weights[:, :, None]
    return jnp.sum(weighted, axis=1)


def side_branch(
    after_mixer, shared_gate, shared_up, shared_down, side_gate, dense_gate, dense_up, dense_down
):
    row_count = after_mixer.shape[0]
    row_piece = lax.all_gather(after_mixer, "ep", axis=0, tiled=True)
    switch = jax.nn.sigmoid(jnp.dot(row_piece, side_gate, preferred_element_type=jnp.float32))
    gate_part = jnp.dot(row_piece, dense_gate, preferred_element_type=jnp.float32)
    up_part = jnp.dot(row_piece, dense_up, preferred_element_type=jnp.float32)
    dense_hidden = (jax.nn.silu(gate_part) * up_part * switch[:, None]).astype(jnp.bfloat16)
    shared_hidden = (
        jax.nn.silu(jnp.dot(after_mixer, shared_gate, preferred_element_type=jnp.float32))
        * jnp.dot(after_mixer, shared_up, preferred_element_type=jnp.float32)
    ).astype(jnp.bfloat16)
    total_rows = dense_hidden.shape[0]
    placed = lax.dynamic_update_slice_in_dim(
        jnp.zeros((total_rows, shared_hidden.shape[1]), jnp.bfloat16),
        shared_hidden,
        lax.axis_index("ep") * row_count,
        0,
    )
    hidden_all = jnp.concatenate([dense_hidden, placed], axis=1)
    down_all = jnp.concatenate([dense_down, shared_down], axis=0)
    own_rows = lax.psum_scatter(
        jnp.dot(hidden_all, down_all, preferred_element_type=jnp.float32),
        ("ep", "tp"),
        scatter_dimension=0,
        tiled=True,
    )
    return lax.all_gather(own_rows.astype(jnp.bfloat16), "tp", axis=0, tiled=True)


def per_device(
    tokens,
    lengths,
    old_state,
    query_weight,
    key_weight,
    value_weight,
    gate_weight,
    head_gain,
    output_weight,
    first_gain,
    expert_ids,
    expert_weights,
    expert_gate,
    expert_up,
    expert_down,
    shared_gate,
    shared_up,
    shared_down,
    side_gate,
    dense_gate,
    dense_up,
    dense_down,
    second_gain,
):
    row_count = tokens.shape[0]
    local_heads = old_state.shape[1]
    head_size = old_state.shape[-1]
    queries = jnp.dot(tokens, query_weight, preferred_element_type=jnp.float32).reshape(
        row_count, local_heads, head_size
    )
    keys_raw = jnp.dot(tokens, key_weight, preferred_element_type=jnp.float32).reshape(
        row_count, local_heads, head_size
    )
    keys_raw = keys_raw * head_size ** (-0.5)
    values = jnp.dot(tokens, value_weight, preferred_element_type=jnp.float32).reshape(
        row_count, local_heads, head_size
    )
    gating = jnp.dot(tokens, gate_weight, preferred_element_type=jnp.float32)
    query_rot = rotate(queries, lengths)
    key_rot = rotate(keys_raw, lengths)
    head_ids = (
        lax.axis_index("tp") * local_heads + jnp.arange(local_heads, dtype=jnp.int32)
    ).astype(jnp.float32)
    decays = 1.0 - jnp.exp2(-2.0 - 10.0 * head_ids / (HEADS - 1))
    new_state = (
        decays[None, :, None, None] * old_state + key_rot[:, :, :, None] * values[:, :, None, :]
    )
    readout = jnp.einsum("thi,thij->thj", query_rot, new_state, precision=lax.Precision.HIGHEST)
    normed = layer_norm(readout, head_gain.reshape(local_heads, head_size))
    mixed = (normed.reshape(row_count, local_heads * head_size) * jax.nn.silu(gating)).astype(
        jnp.bfloat16
    )
    partial_value = jnp.dot(mixed, output_weight, preferred_element_type=jnp.float32)
    branch = lax.psum(partial_value.astype(jnp.bfloat16), "tp").astype(jnp.float32)
    after_mixer = layer_norm(
        RESIDUAL_SCALE * tokens.astype(jnp.float32) + branch, first_gain
    ).astype(jnp.bfloat16)
    routed = route_experts(
        after_mixer, expert_ids, expert_weights, expert_gate, expert_up, expert_down
    )
    side = side_branch(
        after_mixer,
        shared_gate,
        shared_up,
        shared_down,
        side_gate,
        dense_gate,
        dense_up,
        dense_down,
    )
    total = RESIDUAL_SCALE * after_mixer.astype(jnp.float32) + routed + side.astype(jnp.float32)
    layer_out = layer_norm(total, second_gain).astype(jnp.bfloat16)
    return (layer_out, new_state)


def solution(mesh):
    return jax.shard_map(
        per_device,
        mesh=mesh,
        in_specs=(
            P("ep", None),
            P("ep"),
            P("ep", "tp", None, None),
            P(None, "tp"),
            P(None, "tp"),
            P(None, "tp"),
            P(None, "tp"),
            P("tp"),
            P("tp", None),
            P(),
            P("ep", None),
            P("ep", None),
            P("ep", None, "tp"),
            P("ep", None, "tp"),
            P("ep", "tp", None),
            P(None, "tp"),
            P(None, "tp"),
            P("tp", None),
            P(),
            P(None, ("ep", "tp")),
            P(None, ("ep", "tp")),
            P(("ep", "tp"), None),
            P(),
        ),
        out_specs=(P("ep", None), P("ep", "tp", None, None)),
        check_vma=False,
    )
```

profile of v0, /device:TPU:0, one launch (start us, length us, event | category | flops | bytes accessed | tf_op | source)
XLA Modules:
  0.0 191.7 jit_solution(2164469225561733974)
XLA Ops:
  7.3 1.6 convolution_multiply_fusion.2
  8.9 0.7 convert_element_type.61
  9.6 1.5 fusion.43
  11.1 0.2 fusion.44
  11.4 0.1 multiply_cosine_fusion
  11.5 0.1 multiply_subtract_fusion
  11.7 0.1 pad_maximum_fusion
  11.8 2.0 %multiply_add_fusion = f32[16,2,128,128]{3,2,1,0:T(8,128)S(1)} fusion(f32[16,2,128,128]{3,2,1,0:T(8,128)} %param.25, f32[16,2,128]{2,1,0:T(2,128)S(1)} %mul.268, f32[16,2,128]{2,1,0:T(2,128)S(1)} %get-tuple-element.13, f32[2]{0:T(128)S(1)} %exponential_subtract_fusion), kind=kLoop, calls=%fused_computation.5 | loop fusion | flops 1572864 | bytes 4227080 | tf_op jit(solution)/shard_map/add | solution.py:159
  13.8 1.9 fusion.45
  15.7 0.1 reduce_sum.72
  15.8 0.2 multiply_reduce_fusion.2
  16.0 0.1 multiply_multiply_fusion
  16.1 2.9 %convolution_convert_fusion.2 = bf16[16,2048]{1,0:T(8,128)(2,1)} fusion(bf16[256,2048]{1,0:T(8,128)(2,1)} %param.31, f32[2,8,2,128]{3,2,1,0:T(2,128)S(1)} %bitcast.80, bf16[16,2048]{1,0:T(8,128)(2,1)S(1)} %copy-done.2, bf16[2048,256]{1,0:T(8,128)(2,1)} %param.29), kind=kOutput, calls=%fused_computation.4 | convolution fusion | flops 33611776 | bytes 2244608 | tf_op jit(solution)/shard_map/dot_general | solution.py:166
  19.1 0.1 reshape.166
  19.3 0.1 reduce_window_sum.11
  19.4 0.2 select_reduce_fusion
  19.8 33.6 %all-reduce.4.cloned.1.call-done = bf16[16,2048]{1,0:T(8,128)(2,1)} async-done(((bf16[16,2048]{1,0:T(8,128)(2,1)}), bf16[16,2048]{1,0:T(8,128)(2,1)}) %all-reduce.4.cloned.1.call-update) | async-done | bytes 65552 | tf_op jit(solution)/shard_map/psum | solution.py:167
  53.4 1.0 fusion.20
  54.4 1.0 multiply_reduce_fusion.1
  55.5 0.9 multiply_convert_fusion.1
  56.4 31.4 %all_gather.14 = bf16[128,2048]{1,0:T(8,128)(2,1)S(1)} all-gather(bf16[16,2048]{1,0:T(8,128)(2,1)S(1)} %multiply_convert_fusion.1), channel_id=1, replica_groups=mesh['ep'=8,'tp'=4] {'ep'}, dimensions={0}, use_global_device_ids=true | all-gather | bytes 589824 | tf_op jit(solution)/shard_map/all_gather | solution.py:86
  87.8 1.2 fusion.47
  89.1 0.1 reshape.167
  89.2 0.3 convolution_convert_fusion
  89.5 0.2 reshape.168
  89.7 0.7 copy.36
  90.4 5.3 %all-to-all-start = ((bf16[8,2,7,512]{3,1,2,0:T(2,128)(2,1)}), bf16[8,2,7,512]{3,1,2,0:T(2,128)(2,1)S(1)}, u32[]{:S(2)}, u32[]{:S(2)}) async-start(bf16[8,2,7,512]{3,1,2,0:T(2,128)(2,1)} %copy.36), calls=%async_computation | async-start | bytes 229376 | tf_op jit(solution)/shard_map/all_to_all | solution.py:70
  95.8 1.6 fusion.46
  97.5 0.2 fusion.11
  97.7 5.3 %all-to-all-done = bf16[8,2,7,512]{3,1,2,0:T(2,128)(2,1)S(1)} async-done(((bf16[8,2,7,512]{3,1,2,0:T(2,128)(2,1)}), bf16[8,2,7,512]{3,1,2,0:T(2,128)(2,1)S(1)}, u32[]{:S(2)}, u32[]{:S(2)}) %all-to-all-start) | async-done | bytes 114720 | tf_op jit(solution)/shard_map/all_to_all | solution.py:70
  103.0 6.3 %all_gather.12 = bf16[8,2,7,2048]{3,0,2,1:T(8,128)(2,1)S(1)} all-gather(bf16[8,2,7,512]{3,0,2,1:T(8,128)(2,1)S(1)} %copy.37), channel_id=1, replica_groups=mesh['ep'=8,'tp'=4] {'tp'}, dimensions={3}, use_global_device_ids=true | all-gather | bytes 573440 | tf_op jit(solution)/shard_map/all_gather | solution.py:71
  109.3 1.5 convolution_bitcast_fusion.1
  110.9 1.3 fusion
  112.2 0.2 fusion.15
  112.4 1.7 fusion.7
  114.2 0.4 fusion.1
  114.6 49.3 %all-reduce.5 = bf16[128,2048]{1,0:T(8,128)(2,1)S(1)} all-reduce(f32[128,2048]{1,0:T(8,128)S(1)} %fusion.1), channel_id=3, replica_groups=mesh['ep'=8,'tp'=4] {'ep','tp'}, use_global_device_ids=true, to_apply=%region_9.10.clone | all-reduce | flops 262144 | bytes 1572864
  164.0 1.6 copy.38
  165.6 3.7 %all-to-all-start.1 = ((bf16[8,2,7,512]{3,1,2,0:T(2,128)(2,1)}), bf16[8,2,7,512]{3,1,2,0:T(2,128)(2,1)S(1)}, u32[]{:S(2)}, u32[]{:S(2)}) async-start(bf16[8,2,7,512]{3,1,2,0:T(2,128)(2,1)} %copy.38), calls=%async_computation.2 | async-start | bytes 229376 | tf_op jit(solution)/shard_map/all_to_all | solution.py:74
  169.4 5.2 %all-gather = bf16[4,4,2048]{2,1,0:T(4,128)(2,1)S(1)} all-gather(bf16[1,4,2048]{2,1,0:T(4,128)(2,1)S(1)} %fusion.33), channel_id=1, replica_groups=mesh['ep'=8,'tp'=4] {'tp'}, dimensions={0}, use_global_device_ids=true | all-gather | bytes 81920 | tf_op jit(solution)/shard_map/all_gather | solution.py:110
  174.6 2.0 %all-to-all-done.1 = bf16[8,2,7,512]{3,1,2,0:T(2,128)(2,1)S(1)} async-done(((bf16[8,2,7,512]{3,1,2,0:T(2,128)(2,1)}), bf16[8,2,7,512]{3,1,2,0:T(2,128)(2,1)S(1)}, u32[]{:S(2)}, u32[]{:S(2)}) %all-to-all-start.1) | async-done | bytes 114720 | tf_op jit(solution)/shard_map/all_to_all | solution.py:74
  176.6 6.6 %all_gather.13 = bf16[8,2,7,2048]{3,1,2,0:T(2,128)(2,1)S(1)} all-gather(bf16[8,2,7,512]{3,1,2,0:T(2,128)(2,1)S(1)} %all-to-all-done.1), channel_id=1, replica_groups=mesh['ep'=8,'tp'=4] {'tp'}, dimensions={3}, use_global_device_ids=true | all-gather | bytes 573440 | tf_op jit(solution)/shard_map/all_gather | solution.py:75
  183.2 0.2 copy.39
  183.3 0.2 reshape.178
  183.5 0.3 fusion.5
  183.8 0.1 fusion.40
  183.9 0.2 multiply_reduce_fusion
  184.2 0.7 multiply_convert_fusion
  (60 shorter events, 0.8 us)
Async XLA Ops:
  7.2 103.7 %copy-start = (bf16[2,128,2048]{2,1,0:T(8,128)(2,1)S(1)}, bf16[2,128,2048]{2,1,0:T(8,128)(2,1)}, u32[]{:S(2)}) copy-start(bf16[2,128,2048]{2,1,0:T(8,128)(2,1)} %param.37) | copy-start | bytes 3145732
  7.2 3.9 %copy-start.2 = (bf16[16,2048]{1,0:T(8,128)(2,1)S(1)}, bf16[16,2048]{1,0:T(8,128)(2,1)}, u32[]{:S(2)}) copy-start(bf16[16,2048]{1,0:T(8,128)(2,1)} %param.23) | copy-start | bytes 196612
  7.2 3.9 %copy-start.4 = (bf16[2048,256]{1,0:T(8,128)(2,1)S(1)}, bf16[2048,256]{1,0:T(8,128)(2,1)}, u32[]{:S(2)}) copy-start(bf16[2048,256]{1,0:T(8,128)(2,1)} %param.28) | copy-start | bytes 3145732
  7.2 46.2 %all-reduce.4.cloned.1.call-start = ((), (), s32[]{:S(2)}) async-start(), calls=%async_computation.3 | async-start | bytes 131072 | tf_op jit(solution)/shard_map/psum | solution.py:167
  13.7 5.3 %copy-start.1 = (f32[16,2,128,128]{3,2,1,0:T(8,128)}, f32[16,2,128,128]{3,2,1,0:T(8,128)S(1)}, u32[]{:S(2)}) copy-start(f32[16,2,128,128]{3,2,1,0:T(8,128)S(1)} %multiply_add_fusion) | copy-start | bytes 6291460
  13.7 2.2 %copy-start.12 = (f32[256]{0:T(256)S(1)}, f32[256]{0:T(256)}, u32[]{:S(2)}) copy-start(f32[256]{0:T(256)} %param.30) | copy-start | bytes 3076
  13.8 5.3 %copy-start.10 = (s32[16,6]{0,1:T(8,128)S(1)}, s32[16,6]{0,1:T(8,128)}, u32[]{:S(2)}) copy-start(s32[16,6]{0,1:T(8,128)} %param.33) | copy-start | bytes 1156
  13.8 6.0 %copy-start.11 = (bf16[2048]{0:T(1024)(128)(2,1)S(1)}, bf16[2048]{0:T(1024)(128)(2,1)}, u32[]{:S(2)}) copy-start(bf16[2048]{0:T(1024)(128)(2,1)} %param.41) | copy-start | bytes 12292
  13.8 41.7 %copy-start.8 = (f32[2048]{0:T(1024)S(1)}, f32[2048]{0:T(1024)}, u32[]{:S(2)}) copy-start(f32[2048]{0:T(1024)} %param.32) | copy-start | bytes 24580
  89.2 8.2 %copy-start.5 = (bf16[2048,128]{1,0:T(8,128)(2,1)S(1)}, bf16[2048,128]{1,0:T(8,128)(2,1)}, u32[]{:S(2)}) copy-start(bf16[2048,128]{1,0:T(8,128)(2,1)} %param.39) | copy-start | bytes 1572868
  90.4 12.6 %all-to-all-start = ((bf16[8,2,7,512]{3,1,2,0:T(2,128)(2,1)}), bf16[8,2,7,512]{3,1,2,0:T(2,128)(2,1)S(1)}, u32[]{:S(2)}, u32[]{:S(2)}) async-start(bf16[8,2,7,512]{3,1,2,0:T(2,128)(2,1)} %copy.36), calls=%async_computation | async-start | bytes 229376 | tf_op jit(solution)/shard_map/all_to_all | solution.py:70
  95.8 15.1 %copy-start.3 = (bf16[2,2048,128]{2,1,0:T(8,128)(2,1)S(1)}, bf16[2,2048,128]{2,1,0:T(8,128)(2,1)}, u32[]{:S(2)}) copy-start(bf16[2,2048,128]{2,1,0:T(8,128)(2,1)} %param.36) | copy-start | bytes 3145732
  95.8 68.2 %reduce-scatter.2.cloned.1.call-start = ((), (), s32[]{:S(2)}) async-start(), calls=%async_computation.4 | async-start | bytes 573440 | tf_op jit(solution)/shard_map/reduce_scatter | solution.py:73
  97.6 5.4 %copy-start.6 = (bf16[128,128]{1,0:T(8,128)(2,1)}, bf16[128,128]{1,0:T(8,128)(2,1)S(1)}, u32[]{:S(2)}) copy-start(bf16[128,128]{1,0:T(8,128)(2,1)S(1)} %fusion.11) | copy-start | bytes 98308
  112.2 2.0 %copy-start.7 = (bf16[128,128]{1,0:T(8,128)(2,1)S(1)}, bf16[128,128]{1,0:T(8,128)(2,1)}, u32[]{:S(2)}) copy-start(bf16[128,128]{1,0:T(8,128)(2,1)} %copy-done.6) | copy-start | bytes 98308
  112.2 2.0 %copy-start.13 = (bf16[256,2048]{1,0:T(8,128)(2,1)S(1)}, bf16[256,2048]{1,0:T(8,128)(2,1)}, u32[]{:S(2)}) copy-start(bf16[256,2048]{1,0:T(8,128)(2,1)} %param.44) | copy-start | bytes 3145732
  112.2 2.0 %copy-start.14 = (bf16[128,2048]{1,0:T(8,128)(2,1)S(1)}, bf16[128,2048]{1,0:T(8,128)(2,1)}, u32[]{:S(2)}) copy-start(bf16[128,2048]{1,0:T(8,128)(2,1)} %param.40) | copy-start | bytes 1572868
  114.6 68.9 %copy-start.15 = (f32[16,6]{0,1:T(8,128)S(1)}, f32[16,6]{0,1:T(8,128)}, u32[]{:S(2)}) copy-start(f32[16,6]{0,1:T(8,128)} %param.34) | copy-start | bytes 1156
  165.6 11.0 %all-to-all-start.1 = ((bf16[8,2,7,512]{3,1,2,0:T(2,128)(2,1)}), bf16[8,2,7,512]{3,1,2,0:T(2,128)(2,1)S(1)}, u32[]{:S(2)}, u32[]{:S(2)}) async-start(bf16[8,2,7,512]{3,1,2,0:T(2,128)(2,1)} %copy.38), calls=%async_computation.2 | async-start | bytes 229376 | tf_op jit(solution)/shard_map/all_to_all | solution.py:74
  169.3 14.8 %copy-start.9 = (f32[2048]{0:T(1024)S(1)}, f32[2048]{0:T(1024)}, u32[]{:S(2)}) copy-start(f32[2048]{0:T(1024)} %param.45) | copy-start | bytes 24580
Sparse Core Ops, SparseCore 0:
  19.1 34.2 all-reduce.3
  112.3 18.7 reduce-scatter.1
where the time goes:
time: 192 us
  blocking collectives  98.9 us (52%)
  waiting for transfers between devices  41 us (21%)
  matrix products  16.9 us (9%)
  between operations  14.6 us (8%)
  starting transfers between devices  9.12 us (5%)
  other arithmetic  7.84 us (4%)
  local copies, waits for them, and re-layouts  3.44 us (2%)
    unnamed x1, blocking collectives  49.3 us
    psum x1, waiting for transfers between devices, per_device(): lax.psum(partial_value.astype(jnp.bfloat16), 'tp').astype(jnp.float32)  33.6 us
    all_gather x1, blocking collectives, side_branch(): row_piece = lax.all_gather(after_mixer, 'ep', axis=0, tiled=True)  31.4 us
    all_gather x1, blocking collectives, route_experts(): returned = lax.all_gather(came_back, 'tp', axis=3, tiled=True)  6.6 us
    all_gather x1, blocking collectives, route_experts(): whole_rows = lax.all_gather(arrived, 'tp', axis=3, tiled=True)  6.32 us
    all_to_all x1, waiting for transfers between devices, route_experts(): lax.all_to_all(own_cols, 'ep', split_axis=0, concat_axis=0, tiled=True)  5.33 us
    all_to_all x1, starting transfers between devices, route_experts(): lax.all_to_all(own_cols, 'ep', split_axis=0, concat_axis=0, tiled=True)  5.32 us
    all_gather x1, blocking collectives, side_branch(): lax.all_gather(own_rows.astype(jnp.bfloat16), 'tp', axis=0, tiled=True)  5.24 us
  transfers between devices with their start and end apart: 4, of which 3 were waited for; matrix products, arithmetic and copies ran while one was open for 3% of the time, Pallas kernels for 0%

commit v1 on v0

v1 whole, which is shorter than its diff:
```python
import functools

import jax
import jax.numpy as jnp
from jax import lax
from jax.experimental import pallas as pl
from jax.experimental.pallas import tpu as pltpu
from jax.sharding import PartitionSpec as P

MESH = pl.DeviceIdType.MESH
NORM_EPS = 1e-05
RESIDUAL_SCALE = 2.0**0.5
F32 = jnp.float32
BF16 = jnp.bfloat16
LANES = 128


def dot(left, right):
    return jnp.dot(left, right, preferred_element_type=F32)


def silu(x):
    return x * jax.nn.sigmoid(x)


def normalize(x, gain):
    centered = x - jnp.mean(x, axis=-1, keepdims=True)
    variance = jnp.mean(centered * centered, axis=-1, keepdims=True)
    return centered * lax.rsqrt(variance + NORM_EPS) * gain


def mixer_kernel(
    n_tp, tokens, turn_same, turn_other, head_gain, state_hbm, q_hbm, k_hbm, v_hbm, g_hbm, o_hbm,
    share_out, state_out, qw, kw, vw, gw, ow, state, fresh, readout, in_sem, state_sem, out_sem,
):
    rows, heads, size = state.shape[0], state.shape[1], state.shape[2]
    parts = state_sem.shape[0]
    span = rows // parts
    loads = []
    for at, (src, dst) in enumerate(((q_hbm, qw), (k_hbm, kw), (v_hbm, vw))):
        loads.append(pltpu.make_async_copy(src, dst, in_sem.at[at]))
    states = [
        pltpu.make_async_copy(
            state_hbm.at[pl.ds(p * span, span)], state.at[pl.ds(p * span, span)], state_sem.at[p]
        )
        for p in range(parts)
    ]
    late = [
        pltpu.make_async_copy(g_hbm, gw, in_sem.at[3]),
        pltpu.make_async_copy(o_hbm, ow, in_sem.at[4]),
    ]
    for copy in loads + states + late:
        copy.start()
    toks = tokens[...]
    loads[0].wait()
    queries = dot(toks, qw[...])
    loads[1].wait()
    keys = dot(toks, kw[...]) * size**-0.5
    same, other = turn_same[...], turn_other[...]

    def turned(x):
        return x * same + pltpu.roll(x, size // 2, 1) * other

    stack = []
    for h in range(heads):
        stack.append(turned(queries[:, h * size : (h + 1) * size]))
        stack.append(turned(keys[:, h * size : (h + 1) * size]))
    fill = size - 2 * heads * rows
    if fill:
        stack.append(jnp.zeros((fill, size), F32))
    columns = jnp.concatenate(stack, axis=0).T
    loads[2].wait()
    values = dot(toks, vw[...])
    first_head = lax.axis_index("tp") * heads
    decays = []
    for h in range(heads):
        number = (jnp.zeros((1, size), jnp.int32) + (first_head + h)).astype(F32)
        decays.append(1.0 - jnp.exp2(-2.0 - 10.0 * number / (heads * n_tp - 1)))
    writes = []
    for p in range(parts):
        states[p].wait()
        for t in range(p * span, (p + 1) * span):
            for h in range(heads):
                at = 2 * h * rows + t
                new = decays[h] * state[t, h] + columns[:, at + rows : at + rows + 1] * values[
                    t : t + 1, h * size : (h + 1) * size
                ]
                fresh[t, h] = new
                readout[t : t + 1, h * size : (h + 1) * size] = jnp.sum(
                    columns[:, at : at + 1] * new, axis=0, keepdims=True
                )
        write = pltpu.make_async_copy(
            fresh.at[pl.ds(p * span, span)], state_out.at[pl.ds(p * span, span)], out_sem.at[p]
        )
        write.start()
        writes.append(write)
    late[0].wait()
    gating = dot(toks, gw[...])
    late[1].wait()
    total = None
    for h in range(heads):
        cols = slice(h * size, (h + 1) * size)
        mixed = (normalize(readout[:, cols], head_gain[:, cols]) * silu(gating[:, cols])).astype(BF16)
        term = dot(mixed, ow[cols, :])
        total = term if total is None else total + term
    share_out[...] = total.astype(BF16)
    for write in writes:
        write.wait()


def layer_kernel(
    n_ep, n_tp,
    share, tokens, ids, id_weights, first_gain, second_gain, side_gate,
    dg_h, du_h, dd_h, eg_h, eu_h, ed_h, sg_h, su_h, sd_h,
    out,
    dg, du, dd, eg, eu, ed, sg, su, sd,
    got1, gathered, normed, switches, routing, hid_d, hid_e, hid_s, own_sum, core_out, core_in,
    y_out, y_in, total_out, ep_in, final,
    w_sem, s1, r1, sr, rr, sa, ra, sy, ry, sc, rc, s3, r3, s4, r4, s5, r5, s6, r6,
):
    ep, tp = lax.axis_index("ep"), lax.axis_index("tp")
    rows, width = tokens.shape
    cw = width // n_tp
    n_y = n_tp // 2
    y, core = tp // 2, lax.rem(tp, 2)
    mate = y * 2 + 1 - core
    barrier = pltpu.get_barrier_semaphore()

    def greet_ep(d, _):
        pl.semaphore_signal(
            barrier, inc=1, device_id=(lax.rem(ep + d, n_ep), tp), device_id_type=MESH
        )
        return 0

    def greet_tp(d, _):
        pl.semaphore_signal(
            barrier, inc=1, device_id=(ep, lax.rem(tp + d, n_tp)), device_id_type=MESH
        )
        return 0

    lax.fori_loop(1, n_ep, greet_ep, 0)
    lax.fori_loop(1, n_tp, greet_tp, 0)
    weights = [
        pltpu.make_async_copy(src, dst, w_sem.at[at])
        for at, (src, dst) in enumerate(
            ((dg_h, dg), (du_h, du), (eg_h, eg), (eu_h, eu), (sg_h, sg), (su_h, su), (dd_h, dd), (ed_h, ed), (sd_h, sd))
        )
    ]
    for copy in weights:
        copy.start()

    def rows_of(i):
        return pl.ds(pl.multiple_of(i * rows, rows), rows)

    def cols_of(j):
        return pl.ds(pl.multiple_of(j * cw, cw), cw)

    lane = lax.broadcasted_iota(jnp.int32, (rows, LANES), 1)
    mine = jnp.zeros((rows, LANES), F32)
    for k in range(ids.shape[1]):
        mine = mine + jnp.where(ids[:, k : k + 1] == lane, id_weights[:, k : k + 1], 0.0)
    routing[rows_of(ep), :] = mine
    hid_s[...] = jnp.zeros_like(hid_s)
    pl.semaphore_wait(barrier, n_ep + n_tp - 2)

    def copy1(d):
        peer = lax.rem(tp + d, n_tp)
        return pltpu.make_async_remote_copy(
            src_ref=share.at[:, cols_of(peer)], dst_ref=got1.at[d], send_sem=s1.at[d], recv_sem=r1.at[d],
            device_id=(ep, peer), device_id_type=MESH,
        )

    def copy_routing(d):
        return pltpu.make_async_remote_copy(
            src_ref=routing.at[rows_of(ep)], dst_ref=routing.at[rows_of(ep)], send_sem=sr.at[d],
            recv_sem=rr.at[d], device_id=(lax.rem(ep + d, n_ep), tp), device_id_type=MESH,
        )

    def routing_from(d):
        origin = rows_of(lax.rem(ep - d + n_ep, n_ep))
        return pltpu.make_async_remote_copy(
            src_ref=routing.at[origin], dst_ref=routing.at[origin], send_sem=sr.at[d],
            recv_sem=rr.at[d], device_id=(lax.rem(ep + d, n_ep), tp), device_id_type=MESH,
        )

    def loop(low, high, action):
        def step(d, carry):
            action(d)
            return carry

        lax.fori_loop(low, high, step, 0)

    loop(1, n_tp, lambda d: copy1(d).start())
    loop(1, n_ep, lambda d: copy_routing(d).start())
    piece = RESIDUAL_SCALE * tokens[:, cols_of(tp)].astype(F32) + share[:, cols_of(tp)].astype(F32)
    for d in range(1, n_tp):
        copy1(d).wait_recv()
        piece = piece + got1[d].astype(F32)
    gathered[rows_of(ep), cols_of(tp)] = piece.astype(BF16)

    def block(i, j):
        return gathered.at[rows_of(i), cols_of(j)]

    def ag(d, origin):
        return pltpu.make_async_remote_copy(
            src_ref=block(origin, tp), dst_ref=block(origin, tp), send_sem=sa.at[d], recv_sem=ra.at[d],
            device_id=(lax.rem(ep + d, n_ep), tp), device_id_type=MESH,
        )

    def along_y(d, e, j):
        peer = lax.rem(y + e, n_y) * 2 + core
        origin = lax.rem(ep - d + n_ep, n_ep)
        return pltpu.make_async_remote_copy(
            src_ref=block(origin, j), dst_ref=block(origin, j), send_sem=sy.at[e - 1, d],
            recv_sem=ry.at[e - 1, d], device_id=(ep, peer), device_id_type=MESH,
        )

    def to_mate(d, e, side):
        origin = lax.rem(ep - d + n_ep, n_ep)
        j = lax.rem(y - e + n_y, n_y) * 2 + side
        return pltpu.make_async_remote_copy(
            src_ref=block(origin, j), dst_ref=block(origin, j), send_sem=sc.at[e, d],
            recv_sem=rc.at[e, d], device_id=(ep, mate), device_id_type=MESH,
        )

    loop(1, n_ep, lambda d: ag(d, ep).start())

    def pass_on(d):
        for e in range(1, n_y):
            along_y(d, e, tp).start()
        to_mate(d, 0, core).start()

    pass_on(0)

    def arrived(d):
        ag(d, lax.rem(ep - d + n_ep, n_ep)).wait_recv()
        pass_on(d)

    loop(1, n_ep, arrived)

    def over(d):
        for e in range(1, n_y):
            along_y(d, e, lax.rem(y - e + n_y, n_y) * 2 + core).wait_recv()
            to_mate(d, e, core).start()

    loop(0, n_ep, over)

    gain1 = first_gain[...]
    side = side_gate[...].astype(F32)

    def finish(d):
        for e in range(n_y):
            to_mate(d, e, 1 - core).wait_recv()
        where = rows_of(lax.rem(ep - d + n_ep, n_ep))
        after = normalize(gathered[where, :].astype(F32), gain1).astype(BF16)
        normed[where, :] = after
        turned = jax.nn.sigmoid(jnp.sum(after.astype(F32) * side, axis=-1, keepdims=True))
        switches[where, :] = jnp.broadcast_to(turned, (rows, LANES))

    loop(0, n_ep, finish)
    loop(1, n_ep, lambda d: routing_from(d).wait_recv())

    everyone = normed[...]
    weights[0].wait()
    gate = dot(everyone, dg[...])
    weights[1].wait()
    up = dot(everyone, du[...])
    hid_d[...] = (silu(gate) * up * switches[:, 0:1]).astype(BF16)
    weights[2].wait()
    weights[3].wait()
    experts = eg.shape[0]
    lanes = lax.broadcasted_iota(jnp.int32, routing.shape, 1)
    for e in range(experts):
        weight = jnp.sum(
            jnp.where(lanes == ep * experts + e, routing[...], 0.0), axis=-1, keepdims=True
        )
        hid_e[e] = (silu(dot(everyone, eg[e])) * dot(everyone, eu[e]) * weight).astype(BF16)
    weights[4].wait()
    weights[5].wait()
    own = normed[rows_of(ep), :]
    hid_s[rows_of(ep), :] = (silu(dot(own, sg[...])) * dot(own, su[...])).astype(BF16)
    for at in (6, 7, 8):
        weights[at].wait()

    def product(j):
        cols = cols_of(j)
        result = dot(hid_d[...], dd[:, cols]) + dot(hid_s[...], sd[:, cols])
        for e in range(experts):
            result = result + dot(hid_e[e], ed[e, :, cols])
        return result

    def core_copy(e):
        return pltpu.make_async_remote_copy(
            src_ref=core_out.at[e], dst_ref=core_in.at[e], send_sem=s3.at[e], recv_sem=r3.at[e],
            device_id=(ep, mate), device_id_type=MESH,
        )

    def y_copy(e):
        peer = lax.rem(y + e, n_y) * 2 + core
        return pltpu.make_async_remote_copy(
            src_ref=y_out.at[e - 1], dst_ref=y_in.at[e - 1], send_sem=s4.at[e - 1], recv_sem=r4.at[e - 1],
            device_id=(ep, peer), device_id_type=MESH,
        )

    for e in list(range(1, n_y)) + [0]:
        target = lax.rem(y + e, n_y) * 2
        core_out[e] = product(target + 1 - core).astype(BF16)
        core_copy(e).start()
        own_sum[...] = product(target + core)
        core_copy(e).wait_recv()
        if e:
            y_out[e - 1] = (own_sum[...] + core_in[e].astype(F32)).astype(BF16)
            y_copy(e).start()
    total = own_sum[...] + core_in[0].astype(F32)
    for e in range(1, n_y):
        y_copy(e).wait_recv()
        total = total + y_in[e - 1].astype(F32)
    total_out[...] = total.astype(BF16)

    def ep_copy(d):
        peer = lax.rem(ep + d, n_ep)
        return pltpu.make_async_remote_copy(
            src_ref=total_out.at[rows_of(peer)], dst_ref=ep_in.at[d], send_sem=s5.at[d],
            recv_sem=r5.at[d], device_id=(peer, tp), device_id_type=MESH,
        )

    loop(1, n_ep, lambda d: ep_copy(d).start())

    def gather_sum(d, so_far):
        ep_copy(d).wait_recv()
        return so_far + ep_in[d].astype(F32)

    mine = lax.fori_loop(1, n_ep, gather_sum, total_out[rows_of(ep), :].astype(F32))
    final[:, cols_of(tp)] = mine.astype(BF16)

    def last_copy(d, j):
        return pltpu.make_async_remote_copy(
            src_ref=final.at[:, cols_of(j)], dst_ref=final.at[:, cols_of(j)], send_sem=s6.at[d],
            recv_sem=r6.at[d], device_id=(ep, lax.rem(tp + d, n_tp)), device_id_type=MESH,
        )

    loop(1, n_tp, lambda d: last_copy(d, tp).start())
    loop(1, n_tp, lambda d: last_copy(d, lax.rem(tp - d + n_tp, n_tp)).wait_recv())
    result = RESIDUAL_SCALE * normed[rows_of(ep), :].astype(F32) + final[...].astype(F32)
    out[...] = normalize(result, second_gain[...]).astype(BF16)

    def settle(d):
        ag(d, ep).wait_send()
        copy_routing(d).wait_send()
        ep_copy(d).wait_send()

    loop(1, n_ep, settle)

    def settle_tp(d):
        copy1(d).wait_send()
        last_copy(d, tp).wait_send()

    loop(1, n_tp, settle_tp)

    def settle_forward(d):
        for e in range(n_y):
            to_mate(d, e, core).wait_send()
            if e:
                along_y(d, e, tp).wait_send()

    loop(0, n_ep, settle_forward)
    for e in range(n_y):
        core_copy(e).wait_send()
        if e:
            y_copy(e).wait_send()


def per_device(
    n_ep, n_tp,
    tokens, lengths, old_state, query_weight, key_weight, value_weight, gate_weight, head_gain,
    output_weight, first_gain, expert_ids, expert_weights, expert_gate, expert_up, expert_down,
    shared_gate, shared_up, shared_down, side_gate, dense_gate, dense_up, dense_down, second_gain,
):
    rows, width = tokens.shape
    heads, size = old_state.shape[1], old_state.shape[-1]
    half = size // 2
    frequency = 1.0 / 10000.0 ** (jnp.arange(half, dtype=F32) * 2.0 / size)
    angles = lengths.astype(F32)[:, None] * frequency[None, :]
    cosine, sine = jnp.cos(angles), jnp.sin(angles)
    turn_same = jnp.concatenate([cosine, cosine], axis=1)
    turn_other = jnp.concatenate([-sine, sine], axis=1)
    inner = heads * size
    vmem = pl.BlockSpec(memory_space=pltpu.VMEM)
    anywhere = pl.BlockSpec(memory_space=pl.ANY)
    parts = 4
    dma = pltpu.SemaphoreType.DMA
    share, new_state = pl.pallas_call(
        functools.partial(mixer_kernel, n_tp),
        out_shape=(
            jax.ShapeDtypeStruct((rows, width), BF16),
            jax.ShapeDtypeStruct(old_state.shape, F32),
        ),
        in_specs=[vmem] * 4 + [anywhere] * 6,
        out_specs=(vmem, anywhere),
        scratch_shapes=[pltpu.VMEM((width, inner), BF16)] * 4
        + [
            pltpu.VMEM((inner, width), BF16),
            pltpu.VMEM(old_state.shape, F32),
            pltpu.VMEM(old_state.shape, F32),
            pltpu.VMEM((rows, inner), F32),
            dma((5,)),
            dma((parts,)),
            dma((parts,)),
        ],
        name="mixer",
    )(
        tokens, turn_same, turn_other, head_gain.reshape(1, -1), old_state, query_weight, key_weight,
        value_weight, gate_weight, output_weight,
    )
    cw = width // n_tp
    n_y = n_tp // 2
    everyone = rows * n_ep
    big = [dense_gate, dense_up, dense_down, expert_gate, expert_up, expert_down, shared_gate, shared_up, shared_down]
    layer_out = pl.pallas_call(
        functools.partial(layer_kernel, n_ep, n_tp),
        out_shape=jax.ShapeDtypeStruct((rows, width), BF16),
        in_specs=[vmem] * 7 + [anywhere] * len(big),
        out_specs=vmem,
        scratch_shapes=[pltpu.VMEM(w.shape, BF16) for w in big]
        + [
            pltpu.VMEM((n_tp, rows, cw), BF16),
            pltpu.VMEM((everyone, width), BF16),
            pltpu.VMEM((everyone, width), BF16),
            pltpu.VMEM((everyone, LANES), F32),
            pltpu.VMEM((everyone, LANES), F32),
            pltpu.VMEM((everyone, dense_gate.shape[1]), BF16),
            pltpu.VMEM((expert_gate.shape[0], everyone, expert_gate.shape[2]), BF16),
            pltpu.VMEM((everyone, shared_gate.shape[1]), BF16),
            pltpu.VMEM((everyone, cw), F32),
            pltpu.VMEM((n_y, everyone, cw), BF16),
            pltpu.VMEM((n_y, everyone, cw), BF16),
            pltpu.VMEM((n_y - 1, everyone, cw), BF16),
            pltpu.VMEM((n_y - 1, everyone, cw), BF16),
            pltpu.VMEM((everyone, cw), BF16),
            pltpu.VMEM((n_ep, rows, cw), BF16),
            pltpu.VMEM((rows, width), BF16),
            dma((len(big),)),
        ]
        + [dma((n_tp,))] * 2
        + [dma((n_ep,))] * 4
        + [dma((n_y - 1, n_ep))] * 2
        + [dma((n_y, n_ep))] * 2
        + [dma((n_y,))] * 2
        + [dma((n_y - 1,))] * 2
        + [dma((n_ep,))] * 2
        + [dma((n_tp,))] * 2,
        compiler_params=pltpu.CompilerParams(collective_id=0, has_side_effects=True),
        name="layer",
    )(
        share, tokens, expert_ids, expert_weights, first_gain.reshape(1, -1),
        second_gain.reshape(1, -1), side_gate.reshape(1, -1), *big,
    )
    return layer_out, new_state


def solution(mesh):
    return jax.shard_map(
        functools.partial(per_device, mesh.shape["ep"], mesh.shape["tp"]),
        mesh=mesh,
        in_specs=(
            P("ep", None),
            P("ep"),
            P("ep", "tp", None, None),
            P(None, "tp"),
            P(None, "tp"),
            P(None, "tp"),
            P(None, "tp"),
            P("tp"),
            P("tp", None),
            P(),
            P("ep", None),
            P("ep", None),
            P("ep", None, "tp"),
            P("ep", None, "tp"),
            P("ep", "tp", None),
            P(None, "tp"),
            P(None, "tp"),
            P("tp", None),
            P(),
            P(None, ("ep", "tp")),
            P(None, ("ep", "tp")),
            P(("ep", "tp"), None),
            P(),
        ),
        out_specs=(P("ep", None), P("ep", "tp", None, None)),
        check_vma=False,
    )
```

time: 192 us -> 51.7 us (0.27)
  blocking collectives: 98.9 us -> 0 us
  Pallas kernels: 0 us -> 43.7 us
  waiting for transfers between devices: 41 us -> 0 us
  matrix products: 16.9 us -> 0 us
  between operations: 14.6 us -> 0.65 us
  starting transfers between devices: 9.12 us -> 0 us
  other arithmetic: 7.84 us -> 1.46 us
  local copies, waits for them, and re-layouts: 3.44 us -> 5.49 us
    all_gather x4 -> x0, blocking collectives: 49.6 us -> none  [the longest x1 31.4 us: side_branch(): row_piece = lax.all_gather(after_mixer, 'ep', axis=0, tiled=True)]
    unnamed x1 -> x0, blocking collectives: 49.3 us -> none
    pallas_call x0 -> x2, Pallas kernels: none -> 43.7 us  [the longest x1 37.3 us: per_device(): pl.pallas_call(functools.partial(layer_kernel, n_ep, n_tp), out_shape=jax...]
    psum x1 -> x0, waiting for transfers between devices: 33.6 us -> none  [per_device(): lax.psum(partial_value.astype(jnp.bfloat16), 'tp').astype(jnp.float32)]
    dot_general x15 -> x0, matrix products: 16.9 us -> none  [the longest x1 2.93 us: per_device(): jnp.dot(mixed, output_weight, preferred_element_type=jnp.float32)]
    all_to_all x2 -> x0, starting transfers between devices: 9.04 us -> none  [the longest x1 5.32 us: route_experts(): lax.all_to_all(own_cols, 'ep', split_axis=0, concat_axis=0, tiled=True)]
    all_to_all x2 -> x0, waiting for transfers between devices: 7.28 us -> none  [the longest x1 5.33 us: route_experts(): lax.all_to_all(own_cols, 'ep', split_axis=0, concat_axis=0, tiled=True)]
    unnamed x35 -> x3, local copies, waits for them, and re-layouts: 0.2 us -> 4.2 us
  transfers between devices with their start and end apart: 4 -> 0, of which waited for: 3 -> 0; matrix products, arithmetic and copies ran while one was open for 3% -> 0% of each run, Pallas kernels for 0% -> 0%
where the time goes in v1:
time: 51.7 us; the launch traced here: 51.3 us
  Pallas kernels  43.7 us (85%)
  local copies, waits for them, and re-layouts  5.49 us (11%)
  other arithmetic  1.46 us (3%)
  between operations  0.65 us (1%)
    pallas_call x1, Pallas kernels, per_device(): pl.pallas_call(functools.partial(layer_kernel, n_ep, n_tp), out_shape=jax...  37.3 us
    pallas_call x1, Pallas kernels, per_device(): pl.pallas_call(functools.partial(mixer_kernel, n_tp), out_shape=(jax.Shap...  6.44 us
    unnamed x3, local copies, waits for them, and re-layouts  4.2 us
    reshape x1, local copies, waits for them, and re-layouts, per_device(): side_gate.reshape(1, -1)  1.29 us

profile of v1, /device:TPU:0, one launch (start us, length us, event | category | flops | bytes accessed | tf_op | source)
XLA Modules:
  0.0 51.3 jit_solution(17842222643957538000)
XLA Ops:
  0.6 0.7 %convert_element_type.3 = f32[16]{0:T(128)S(1)} convert(s32[16]{0:T(128)} %param.24) | non-fusion elementwise | flops 16 | bytes 128 | tf_op jit(solution)/shard_map/convert_element_type | solution.py:383
  1.3 1.4 %copy.25.ids = s32[16,6]{1,0:T(8,128)} copy(s32[16,6]{0,1:T(8,128)} %param.33) | data formatting | bytes 768 | tf_op args[10]
  2.7 1.4 %copy.26.id_weights = f32[16,6]{1,0:T(8,128)} copy(f32[16,6]{0,1:T(8,128)} %param.34) | data formatting | bytes 768 | tf_op args[11]
  4.0 1.3 %reshape.26.side_gate = bf16[1,2048]{1,0:T(2,128)(2,1)} reshape(bf16[2048]{0:T(1024)(128)(2,1)} %param.41) | data formatting | bytes 8192 | tf_op jit(solution)/shard_map/reshape | solution.py:456
  5.3 0.1 fusion
  5.4 0.7 %pad_maximum_fusion = (f32[16,128]{1,0:T(8,128)}, f32[16,128]{1,0:T(8,128)}) fusion(f32[16,64]{1,0:T(8,128)S(1)} %get-tuple-element.8, f32[16,64]{1,0:T(8,128)S(1)} %get-tuple-element.7, f32[16,64]{1,0:T(8,128)S(1)} %get-tuple-element.6), kind=kLoop, calls=%fused_computation.2 | loop fusion | flops 4096 | bytes 28672 | tf_op jit(solution)/shard_map/concatenate | solution.py:385
  6.1 6.4 %mixer.1 = (bf16[16,2048]{1,0:T(8,128)(2,1)}, f32[16,2,128,128]{3,2,1,0:T(8,128)}) custom-call(bf16[16,2048]{1,0:T(8,128)(2,1)} %tokens.3, f32[16,128]{1,0:T(8,128)} %get-tuple-element.9.turn_same, f32[16,128]{1,0:T(8,128)} %get-tuple-element.10.turn_other, f32[1,256]{1,0:T(1,128)} %bitcast.5, f32[16,2,128,128]{3,2,1,0:T(8,128)} %state_hbm.1, ...), custom_call_target="tpu_custom_call" | custom-call | tf_op jit(solution)/shard_map/mixer/pallas_call | solution.py:392
  12.6 37.3 %layer.1 = bf16[16,2048]{1,0:T(8,128)(2,1)} custom-call(bf16[16,2048]{1,0:T(8,128)(2,1)} %get-tuple-element.4.share, bf16[16,2048]{1,0:T(8,128)(2,1)} %tokens.3, s32[16,6]{1,0:T(8,128)} %copy.25.ids, f32[16,6]{1,0:T(8,128)} %copy.26.id_weights, f32[1,2048]{1,0:T(1,128)} %bitcast.3, f32[1,2048]{1,0:T(1,128)} %bitcast.4, bf16[1,2048]{1,0:T(2,128)(2,1)} %reshape.26.side_gate, ...), custom_call_target="tpu_custom_call" | custom-call | tf_op jit(solution)/shard_map/layer/pallas_call | solution.py:419
  49.9 1.5 %copy.28 = bf16[16,2048]{1,0:T(8,128)(2,1)} copy(bf16[16,2048]{1,0:T(8,128)(2,1)} %layer.1) | data formatting | bytes 131072
  (1 shorter events, 0.0 us)

commit v2 on v1

--- a/solution.py
+++ b/solution.py
@@ -2,6 +2,7 @@
 
 import jax
 import jax.numpy as jnp
+import numpy as np
 from jax import lax
 from jax.experimental import pallas as pl
 from jax.experimental.pallas import tpu as pltpu
@@ -30,7 +31,7 @@
 
 
 def mixer_kernel(
-    n_tp, tokens, turn_same, turn_other, head_gain, state_hbm, q_hbm, k_hbm, v_hbm, g_hbm, o_hbm,
+    n_tp, lengths, tokens, frequency, head_gain, state_hbm, q_hbm, k_hbm, v_hbm, g_hbm, o_hbm,
     share_out, state_out, qw, kw, vw, gw, ow, state, fresh, readout, in_sem, state_sem, out_sem,
 ):
     rows, heads, size = state.shape[0], state.shape[1], state.shape[2]
@@ -52,11 +53,19 @@
     for copy in loads + states + late:
         copy.start()
     toks = tokens[...]
+    positions = jnp.concatenate(
+        [jnp.zeros((1, size), jnp.int32) + lengths[t] for t in range(rows)], axis=0
+    ).astype(F32)
+    angles = positions * frequency[...]
+    turns = jnp.floor(angles * (0.5 / np.pi) + 0.5)
+    angles = (angles - turns * 6.28125) - turns * (2.0 * np.pi - 6.28125)
+    sine = jnp.sin(angles)
+    first = lax.broadcasted_iota(jnp.int32, (rows, size), 1) < size // 2
+    same, other = jnp.cos(angles), jnp.where(first, -sine, sine)
     loads[0].wait()
     queries = dot(toks, qw[...])
     loads[1].wait()
     keys = dot(toks, kw[...]) * size**-0.5
-    same, other = turn_same[...], turn_other[...]
 
     def turned(x):
         return x * same + pltpu.roll(x, size // 2, 1) * other
@@ -155,10 +164,16 @@
     def cols_of(j):
         return pl.ds(pl.multiple_of(j * cw, cw), cw)
 
-    lane = lax.broadcasted_iota(jnp.int32, (rows, LANES), 1)
-    mine = jnp.zeros((rows, LANES), F32)
-    for k in range(ids.shape[1]):
-        mine = mine + jnp.where(ids[:, k : k + 1] == lane, id_weights[:, k : k + 1], 0.0)
+    number = lax.broadcasted_iota(jnp.int32, (LANES, rows), 0)
+    columns = jnp.zeros((LANES, rows), F32)
+    for k in range(ids.shape[0]):
+        columns = columns + jnp.where(ids[k : k + 1, :] == number, id_weights[k : k + 1, :], 0.0)
+    unit = (
+        lax.broadcasted_iota(jnp.int32, (rows, rows), 0) == lax.broadcasted_iota(jnp.int32, (rows, rows), 1)
+    ).astype(F32)
+    mine = lax.dot_general(
+        unit, columns, (((1,), (1,)), ((), ())), precision=lax.Precision.HIGHEST, preferred_element_type=F32
+    )
     routing[rows_of(ep), :] = mine
     hid_s[...] = jnp.zeros_like(hid_s)
     pl.semaphore_wait(barrier, n_ep + n_tp - 2)
@@ -247,6 +262,7 @@
 
     gain1 = first_gain[...]
     side = side_gate[...].astype(F32)
+    side = jnp.concatenate([side[r : r + 1, :] for r in range(width // LANES)], axis=1)
 
     def finish(d):
         for e in range(n_y):
@@ -282,40 +298,35 @@
     for at in (6, 7, 8):
         weights[at].wait()
 
-    def product(j):
-        cols = cols_of(j)
-        result = dot(hid_d[...], dd[:, cols]) + dot(hid_s[...], sd[:, cols])
+    near_ep = n_ep // 2
+    half_rows = near_ep * rows
+    near = ep // near_ep
+
+    def half_of(s):
+        which = near if s else 1 - near
+        return pl.ds(pl.multiple_of(which * half_rows, half_rows), half_rows)
+
+    def product(s, j):
+        where, cols = half_of(s), cols_of(j)
+        result = dot(hid_d[where, :], dd[:, cols]) + dot(hid_s[where, :], sd[:, cols])
         for e in range(experts):
-            result = result + dot(hid_e[e], ed[e, :, cols])
+            result = result + dot(hid_e[e, where, :], ed[e, :, cols])
         return result
 
-    def core_copy(e):
-        return pltpu.make_async_remote_copy(
-            src_ref=core_out.at[e], dst_ref=core_in.at[e], send_sem=s3.at[e], recv_sem=r3.at[e],
+    def core_copy(s, e):
+        at = s * n_y + e
+        return pltpu.make_async_remote_copy(
+            src_ref=core_out.at[at], dst_ref=core_in.at[at], send_sem=s3.at[at], recv_sem=r3.at[at],
             device_id=(ep, mate), device_id_type=MESH,
         )
 
-    def y_copy(e):
+    def y_copy(s, e):
+        at = s * (n_y - 1) + e - 1
         peer = lax.rem(y + e, n_y) * 2 + core
         return pltpu.make_async_remote_copy(
-            src_ref=y_out.at[e - 1], dst_ref=y_in.at[e - 1], send_sem=s4.at[e - 1], recv_sem=r4.at[e - 1],
+            src_ref=y_out.at[at], dst_ref=y_in.at[at], send_sem=s4.at[at], recv_sem=r4.at[at],
             device_id=(ep, peer), device_id_type=MESH,
         )
-
-    for e in list(range(1, n_y)) + [0]:
-        target = lax.rem(y + e, n_y) * 2
-        core_out[e] = product(target + 1 - core).astype(BF16)
-        core_copy(e).start()
-        own_sum[...] = product(target + core)
-        core_copy(e).wait_recv()
-        if e:
-            y_out[e - 1] = (own_sum[...] + core_in[e].astype(F32)).astype(BF16)
-            y_copy(e).start()
-    total = own_sum[...] + core_in[0].astype(F32)
-    for e in range(1, n_y):
-        y_copy(e).wait_recv()
-        total = total + y_in[e - 1].astype(F32)
-    total_out[...] = total.astype(BF16)
 
     def ep_copy(d):
         peer = lax.rem(ep + d, n_ep)
@@ -324,7 +335,40 @@
             recv_sem=r5.at[d], device_id=(peer, tp), device_id_type=MESH,
         )
 
-    loop(1, n_ep, lambda d: ep_copy(d).start())
+    def terms(s, e):
+        target = lax.rem(y + e, n_y) * 2
+        at = s * n_y + e
+        core_out[at] = product(s, target + 1 - core).astype(BF16)
+        core_copy(s, e).start()
+        own_sum[s] = product(s, target + core)
+        if e:
+            core_copy(s, e).wait_recv()
+            y_out[s * (n_y - 1) + e - 1] = (own_sum[s] + core_in[at].astype(F32)).astype(BF16)
+            y_copy(s, e).start()
+
+    def send_total(s):
+        core_copy(s, 0).wait_recv()
+        total = own_sum[s] + core_in[s * n_y].astype(F32)
+        for e in range(1, n_y):
+            y_copy(s, e).wait_recv()
+            total = total + y_in[s * (n_y - 1) + e - 1].astype(F32)
+        total_out[half_of(s), :] = total.astype(BF16)
+        if s:
+            base = near * near_ep
+            inside = ep - base
+            loop(1, near_ep, lambda m: ep_copy(lax.rem(base + lax.rem(inside + m, near_ep) - ep + n_ep, n_ep)).start())
+        else:
+            base = (1 - near) * near_ep
+            loop(0, near_ep, lambda m: ep_copy(lax.rem(base + m - ep + n_ep, n_ep)).start())
+
+    for e in range(1, n_y):
+        terms(0, e)
+    terms(0, 0)
+    for e in range(1, n_y):
+        terms(1, e)
+    send_total(0)
+    terms(1, 0)
+    send_total(1)
 
     def gather_sum(d, so_far):
         ep_copy(d).wait_recv()
@@ -364,10 +408,11 @@
                 along_y(d, e, tp).wait_send()
 
     loop(0, n_ep, settle_forward)
-    for e in range(n_y):
-        core_copy(e).wait_send()
-        if e:
-            y_copy(e).wait_send()
+    for s in range(2):
+        for e in range(n_y):
+            core_copy(s, e).wait_send()
+            if e:
+                y_copy(s, e).wait_send()
 
 
 def per_device(
@@ -379,11 +424,7 @@
     rows, width = tokens.shape
     heads, size = old_state.shape[1], old_state.shape[-1]
     half = size // 2
-    frequency = 1.0 / 10000.0 ** (jnp.arange(half, dtype=F32) * 2.0 / size)
-    angles = lengths.astype(F32)[:, None] * frequency[None, :]
-    cosine, sine = jnp.cos(angles), jnp.sin(angles)
-    turn_same = jnp.concatenate([cosine, cosine], axis=1)
-    turn_other = jnp.concatenate([-sine, sine], axis=1)
+    frequency = np.tile(10000.0 ** (-np.arange(half) * 2.0 / size), 2)[None].astype(np.float32)
     inner = heads * size
     vmem = pl.BlockSpec(memory_space=pltpu.VMEM)
     anywhere = pl.BlockSpec(memory_space=pl.ANY)
@@ -395,7 +436,7 @@
             jax.ShapeDtypeStruct((rows, width), BF16),
             jax.ShapeDtypeStruct(old_state.shape, F32),
         ),
-        in_specs=[vmem] * 4 + [anywhere] * 6,
+        in_specs=[pl.BlockSpec(memory_space=pltpu.SMEM)] + [vmem] * 3 + [anywhere] * 6,
         out_specs=(vmem, anywhere),
         scratch_shapes=[pltpu.VMEM((width, inner), BF16)] * 4
         + [
@@ -409,7 +450,7 @@
         ],
         name="mixer",
     )(
-        tokens, turn_same, turn_other, head_gain.reshape(1, -1), old_state, query_weight, key_weight,
+        lengths, tokens, jnp.asarray(frequency), head_gain.reshape(1, -1), old_state, query_weight, key_weight,
         value_weight, gate_weight, output_weight,
     )
     cw = width // n_tp
@@ -431,11 +472,11 @@
             pltpu.VMEM((everyone, dense_gate.shape[1]), BF16),
             pltpu.VMEM((expert_gate.shape[0], everyone, expert_gate.shape[2]), BF16),
             pltpu.VMEM((everyone, shared_gate.shape[1]), BF16),
-            pltpu.VMEM((everyone, cw), F32),
-            pltpu.VMEM((n_y, everyone, cw), BF16),
-            pltpu.VMEM((n_y, everyone, cw), BF16),
-            pltpu.VMEM((n_y - 1, everyone, cw), BF16),
-            pltpu.VMEM((n_y - 1, everyone, cw), BF16),
+            pltpu.VMEM((2, everyone // 2, cw), F32),
+            pltpu.VMEM((2 * n_y, everyone // 2, cw), BF16),
+            pltpu.VMEM((2 * n_y, everyone // 2, cw), BF16),
+            pltpu.VMEM((2 * (n_y - 1), everyone // 2, cw), BF16),
+            pltpu.VMEM((2 * (n_y - 1), everyone // 2, cw), BF16),
             pltpu.VMEM((everyone, cw), BF16),
             pltpu.VMEM((n_ep, rows, cw), BF16),
             pltpu.VMEM((rows, width), BF16),
@@ -445,15 +486,15 @@
         + [dma((n_ep,))] * 4
         + [dma((n_y - 1, n_ep))] * 2
         + [dma((n_y, n_ep))] * 2
-        + [dma((n_y,))] * 2
-        + [dma((n_y - 1,))] * 2
+        + [dma((2 * n_y,))] * 2
+        + [dma((2 * (n_y - 1),))] * 2
         + [dma((n_ep,))] * 2
         + [dma((n_tp,))] * 2,
         compiler_params=pltpu.CompilerParams(collective_id=0, has_side_effects=True),
         name="layer",
     )(
-        share, tokens, expert_ids, expert_weights, first_gain.reshape(1, -1),
-        second_gain.reshape(1, -1), side_gate.reshape(1, -1), *big,
+        share, tokens, expert_ids.T, expert_weights.T, first_gain.reshape(1, -1),
+        second_gain.reshape(1, -1), side_gate.reshape(-1, LANES), *big,
     )
     return layer_out, new_state
 

time: 51.7 us -> 44.8 us (0.87)
  local copies, waits for them, and re-layouts: 5.49 us -> 1.47 us
  other arithmetic: 1.46 us -> 0 us
  Pallas kernels: 43.7 us -> 42.4 us
    unnamed x3 -> x1, local copies, waits for them, and re-layouts: 4.2 us -> 1.47 us
    pallas_call x1, Pallas kernels: 37.3 us -> 36 us  [per_device(): pl.pallas_call(functools.partial(layer_kernel, n_ep, n_tp), out_shape=jax...]
    reshape x1 -> x0, local copies, waits for them, and re-layouts: 1.29 us -> none  [per_device(): side_gate.reshape(1, -1)]
    concatenate x1 -> x0, other arithmetic: 0.67 us -> none  [per_device(): turn_same = jnp.concatenate([cosine, cosine], axis=1)]
    convert_element_type x1 -> x0, other arithmetic: 0.66 us -> none  [per_device(): angles = lengths.astype(F32)[:, None] * frequency[None, :]]
where the time goes in v2:
time: 44.8 us; the launch traced here: 44.5 us
  Pallas kernels  42.4 us (95%)
  local copies, waits for them, and re-layouts  1.47 us (3%)
  between operations  0.65 us (1%)
    pallas_call x1, Pallas kernels, per_device(): pl.pallas_call(functools.partial(layer_kernel, n_ep, n_tp), out_shape=jax...  36 us
    pallas_call x1, Pallas kernels, per_device(): pl.pallas_call(functools.partial(mixer_kernel, n_tp), out_shape=(jax.Shap...  6.45 us
    unnamed x1, local copies, waits for them, and re-layouts  1.47 us

profile of v2, /device:TPU:0, one launch (start us, length us, event | category | flops | bytes accessed | tf_op | source)
XLA Modules:
  0.0 44.5 jit_solution(3263473561116932668)
XLA Ops:
  0.6 6.4 %mixer.1 = (bf16[16,2048]{1,0:T(8,128)(2,1)}, f32[16,2,128,128]{3,2,1,0:T(8,128)}) custom-call(s32[16]{0:T(128)} %lengths.1, bf16[16,2048]{1,0:T(8,128)(2,1)} %tokens.3, f32[1,128]{1,0:T(1,128)} %constant.2.clone.frequency, f32[1,256]{1,0:T(1,128)} %bitcast.11, f32[16,2,128,128]{3,2,1,0:T(8,128)} %state_hbm.1, bf16[2048,256]{1,0:T(8,128)(2,1)} %q_hbm.1, ...), custom_call_target="tpu_custom_call" | custom-call | tf_op jit(solution)/shard_map/mixer/pallas_call | solution.py:433
  7.1 36.0 %layer.1 = bf16[16,2048]{1,0:T(8,128)(2,1)} custom-call(bf16[16,2048]{1,0:T(8,128)(2,1)} %get-tuple-element.4.share, bf16[16,2048]{1,0:T(8,128)(2,1)} %tokens.3, s32[6,16]{1,0:T(8,128)} %bitcast.8, f32[6,16]{1,0:T(8,128)} %bitcast.9, f32[1,2048]{1,0:T(1,128)} %bitcast.6, f32[1,2048]{1,0:T(1,128)} %bitcast.7, bf16[16,128]{1,0:T(8,128)(2,1)} %bitcast.10, ...), custom_call_target="tpu_custom_call" | custom-call | tf_op jit(solution)/shard_map/layer/pallas_call | solution.py:460
  43.1 1.5 %copy.27 = bf16[16,2048]{1,0:T(8,128)(2,1)} copy(bf16[16,2048]{1,0:T(8,128)(2,1)} %layer.1) | data formatting | bytes 131072

commit v3 on v2

--- a/solution.py
+++ b/solution.py
@@ -149,14 +149,29 @@
 
     lax.fori_loop(1, n_ep, greet_ep, 0)
     lax.fori_loop(1, n_tp, greet_tp, 0)
+    wide = eg.shape[-1] != eg_h.shape[-1]
+    if wide:
+        unit_e, unit_s = eg_h.shape[-1], sg_h.shape[-1]
+        eg_d, eu_d = eg.at[:, :, pl.ds(0, unit_e)], eg.at[:, :, pl.ds(unit_e, unit_e)]
+        sg_d, su_d = sg.at[:, pl.ds(0, unit_s)], sg.at[:, pl.ds(unit_s, unit_s)]
+    else:
+        eg_d, eu_d, sg_d, su_d = eg, eu, sg, su
+
+    def both(x, gate_ref, up_ref, index):
+        if wide:
+            pair = dot(x, gate_ref[index])
+            middle = pair.shape[1] // 2
+            return silu(pair[:, :middle]) * pair[:, middle:]
+        return silu(dot(x, gate_ref[index])) * dot(x, up_ref[index])
+
     weights = [
         pltpu.make_async_copy(src, dst, w_sem.at[at])
         for at, (src, dst) in enumerate(
-            ((dg_h, dg), (du_h, du), (eg_h, eg), (eu_h, eu), (sg_h, sg), (su_h, su), (dd_h, dd), (ed_h, ed), (sd_h, sd))
+            ((dg_h, dg), (du_h, du), (eg_h, eg_d), (eu_h, eu_d), (sg_h, sg_d), (su_h, su_d), (dd_h, dd), (ed_h, ed), (sd_h, sd))
         )
     ]
-    for copy in weights:
-        copy.start()
+    for at in (4, 5, 0, 1, 2, 3, 6, 7, 8):
+        weights[at].start()
 
     def rows_of(i):
         return pl.ds(pl.multiple_of(i * rows, rows), rows)
@@ -258,8 +273,6 @@
             along_y(d, e, lax.rem(y - e + n_y, n_y) * 2 + core).wait_recv()
             to_mate(d, e, core).start()
 
-    loop(0, n_ep, over)
-
     gain1 = first_gain[...]
     side = side_gate[...].astype(F32)
     side = jnp.concatenate([side[r : r + 1, :] for r in range(width // LANES)], axis=1)
@@ -273,7 +286,14 @@
         turned = jax.nn.sigmoid(jnp.sum(after.astype(F32) * side, axis=-1, keepdims=True))
         switches[where, :] = jnp.broadcast_to(turned, (rows, LANES))
 
-    loop(0, n_ep, finish)
+    loop(0, n_ep - 2, over)
+    finish(0)
+    weights[4].wait()
+    weights[5].wait()
+    own = normed[rows_of(ep), :]
+    hid_s[rows_of(ep), :] = both(own, sg, su, Ellipsis).astype(BF16)
+    loop(n_ep - 2, n_ep, over)
+    loop(1, n_ep, finish)
     loop(1, n_ep, lambda d: routing_from(d).wait_recv())
 
     everyone = normed[...]
@@ -290,11 +310,11 @@
         weight = jnp.sum(
             jnp.where(lanes == ep * experts + e, routing[...], 0.0), axis=-1, keepdims=True
         )
-        hid_e[e] = (silu(dot(everyone, eg[e])) * dot(everyone, eu[e]) * weight).astype(BF16)
-    weights[4].wait()
-    weights[5].wait()
-    own = normed[rows_of(ep), :]
-    hid_s[rows_of(ep), :] = (silu(dot(own, sg[...])) * dot(own, su[...])).astype(BF16)
+        hidden = (both(everyone, eg, eu, e) * weight).astype(BF16)
+        if wide:
+            hid_e[0, :, e * unit_e : (e + 1) * unit_e] = hidden
+        else:
+            hid_e[e] = hidden
     for at in (6, 7, 8):
         weights[at].wait()
 
@@ -309,7 +329,7 @@
     def product(s, j):
         where, cols = half_of(s), cols_of(j)
         result = dot(hid_d[where, :], dd[:, cols]) + dot(hid_s[where, :], sd[:, cols])
-        for e in range(experts):
+        for e in range(ed.shape[0]):
             result = result + dot(hid_e[e, where, :], ed[e, :, cols])
         return result
 
@@ -456,13 +476,21 @@
     cw = width // n_tp
     n_y = n_tp // 2
     everyone = rows * n_ep
+    experts, unit = expert_gate.shape[0], expert_gate.shape[2]
+    wide = unit % LANES == 0
+    if wide:
+        expert_down = expert_down.reshape(1, experts * unit, width)
     big = [dense_gate, dense_up, dense_down, expert_gate, expert_up, expert_down, shared_gate, shared_up, shared_down]
+    shapes = [w.shape for w in big]
+    if wide:
+        shapes[3], shapes[4] = (experts, width, 2 * unit), (16, LANES)
+        shapes[6], shapes[7] = (width, 2 * shared_gate.shape[1]), (16, LANES)
     layer_out = pl.pallas_call(
         functools.partial(layer_kernel, n_ep, n_tp),
         out_shape=jax.ShapeDtypeStruct((rows, width), BF16),
         in_specs=[vmem] * 7 + [anywhere] * len(big),
         out_specs=vmem,
-        scratch_shapes=[pltpu.VMEM(w.shape, BF16) for w in big]
+        scratch_shapes=[pltpu.VMEM(shape, BF16) for shape in shapes]
         + [
             pltpu.VMEM((n_tp, rows, cw), BF16),
             pltpu.VMEM((everyone, width), BF16),
@@ -470,7 +498,7 @@
             pltpu.VMEM((everyone, LANES), F32),
             pltpu.VMEM((everyone, LANES), F32),
             pltpu.VMEM((everyone, dense_gate.shape[1]), BF16),
-            pltpu.VMEM((expert_gate.shape[0], everyone, expert_gate.shape[2]), BF16),
+            pltpu.VMEM((expert_down.shape[0], everyone, expert_down.shape[1]), BF16),
             pltpu.VMEM((everyone, shared_gate.shape[1]), BF16),
             pltpu.VMEM((2, everyone // 2, cw), F32),
             pltpu.VMEM((2 * n_y, everyone // 2, cw), BF16),

time: 44.8 us -> 44.9 us (level)
  no operation moved by 1% of the time
where the time goes in v3:
time: 44.9 us; the launch traced here: 44.6 us
  Pallas kernels  42.5 us (95%)
  local copies, waits for them, and re-layouts  1.47 us (3%)
  between operations  0.65 us (1%)
    pallas_call x1, Pallas kernels, per_device(): pl.pallas_call(functools.partial(layer_kernel, n_ep, n_tp), out_shape=jax...  36 us
    pallas_call x1, Pallas kernels, per_device(): pl.pallas_call(functools.partial(mixer_kernel, n_tp), out_shape=(jax.Shap...  6.45 us
    unnamed x1, local copies, waits for them, and re-layouts  1.47 us

profile of v3, /device:TPU:0, one launch (start us, length us, event | category | flops | bytes accessed | tf_op | source)
XLA Modules:
  0.0 44.6 jit_solution(17658746403785023307)
XLA Ops:
  0.6 6.4 %mixer.1 = (bf16[16,2048]{1,0:T(8,128)(2,1)}, f32[16,2,128,128]{3,2,1,0:T(8,128)}) custom-call(s32[16]{0:T(128)} %lengths.1, bf16[16,2048]{1,0:T(8,128)(2,1)} %tokens.3, f32[1,128]{1,0:T(1,128)} %constant.2.clone.frequency, f32[1,256]{1,0:T(1,128)} %bitcast.13, f32[16,2,128,128]{3,2,1,0:T(8,128)} %state_hbm.1, bf16[2048,256]{1,0:T(8,128)(2,1)} %q_hbm.1, ...), custom_call_target="tpu_custom_call" | custom-call | tf_op jit(solution)/shard_map/mixer/pallas_call | solution.py:453
  7.1 36.0 %layer.1 = bf16[16,2048]{1,0:T(8,128)(2,1)} custom-call(bf16[16,2048]{1,0:T(8,128)(2,1)} %get-tuple-element.4.share, bf16[16,2048]{1,0:T(8,128)(2,1)} %tokens.3, s32[6,16]{1,0:T(8,128)} %bitcast.10, f32[6,16]{1,0:T(8,128)} %bitcast.11, f32[1,2048]{1,0:T(1,128)} %bitcast.8, f32[1,2048]{1,0:T(1,128)} %bitcast.9, bf16[16,128]{1,0:T(8,128)(2,1)} %bitcast.12, ...), custom_call_target="tpu_custom_call" | custom-call | tf_op jit(solution)/shard_map/layer/pallas_call | solution.py:488
  43.1 1.5 %copy.27 = bf16[16,2048]{1,0:T(8,128)(2,1)} copy(bf16[16,2048]{1,0:T(8,128)(2,1)} %layer.1) | data formatting | bytes 131072
